TPU v7x, 32 devices: a whole 2x2x4 slice. The times are simulated.
32 devices in a mesh: ep: 8 (over z, core), tp: 4 (over y, x).
Axes of the slice: x: 2, y: 2, z: 4, core: 2. Of those that a mesh axis runs over, the one named last changes fastest.
Arguments:
- tokens: bfloat16 [128, 4096], P('ep', 'tp'), may hold values from -40 to 40
- norm_gain: bfloat16 [4096], P('tp'), may hold values from 0.099609375 to 1.8984375
- routes: int32 [128, 4], P('ep'), may hold values from 0 to 7, all different within a row; in each aligned block of 16 rows (0 to 15, 16 to 31, ...) at most 16 rows name the same one
- route_weights: float32 [128, 4], P('ep'), may hold values from 0.05 to 1
- w_gate: bfloat16 [8, 4096, 4096], P('ep', None, 'tp'), may hold values from -0.25 to 0.25
- w_up: bfloat16 [8, 4096, 4096], P('ep', None, 'tp'), may hold values from -0.25 to 0.25
- w_down: bfloat16 [8, 4096, 4096], P('ep', 'tp'), may hold values from -0.0234375 to 0.0234375
Outputs:
- mixed: bfloat16 [128, 4096], P('ep', 'tp')
Inputs may be any that keep to these rules, and one draw needn't show every extreme that they name: `routes`: within the 16 rows of one device, each token names 4 different experts, and no expert is named by more than 16 rows; some expert reaches 16.
All inputs are finite; a program needn't handle non-finite values.
Results may differ from a plain program's by a relative error of at most 0.018.
Values may be sent and summed in bfloat16 or wider, within the bound.
No kernel may reach another device: no remote copies, remote signals or barrier semaphores. Data moves between devices by JAX's collectives and lax.ppermute only.
A program may use at most 64 MiB of HBM per device.

v0:
```python
import jax
import jax.numpy as jnp
from jax import lax
from jax.sharding import PartitionSpec as P


def shards(tokens, norm_gain, routes, route_weights, w_gate, w_up, w_down):
    tok_rows = tokens.shape[0]
    topk = routes.shape[1]
    groups = lax.axis_size("ep")
    capacity = min(tok_rows, max(2, 2 * tok_rows * topk // groups))
    slot_rows = groups * capacity
    flat = routes.reshape(-1)
    order = jnp.arange(flat.shape[0], dtype=jnp.int32)
    earlier = (flat[:, None] == flat[None, :]) & (order[:, None] > order[None, :])
    slot = jnp.sum(earlier.astype(jnp.int32), axis=1)
    target = (flat * capacity + slot).reshape(tok_rows, topk)
    slot_ids = jnp.arange(slot_rows, dtype=jnp.int32)
    picker = jnp.any(target[None, :, :] == slot_ids[:, None, None], axis=2).astype(jnp.bfloat16)
    combine = jnp.sum(
        jnp.where(target[:, :, None] == slot_ids[None, None, :], route_weights[:, :, None], 0.0),
        axis=1,
    )
    whole, gain_whole = (
        lax.all_gather(tokens, "tp", axis=1, tiled=True),
        lax.all_gather(norm_gain.reshape(1, -1), "tp", axis=1, tiled=True),
    )
    full_values = whole.astype(jnp.float32)
    scale = lax.rsqrt(jnp.mean(full_values * full_values, axis=1, keepdims=True) + 1e-05)
    normed = (full_values * scale * gain_whole.astype(jnp.float32)).astype(jnp.bfloat16)
    outbound = jnp.dot(picker, normed, preferred_element_type=jnp.float32).astype(jnp.bfloat16)
    arrived = lax.all_to_all(
        outbound.reshape(groups, capacity, -1), "ep", split_axis=0, concat_axis=0, tiled=True
    ).reshape(slot_rows, -1)
    gate_pre = jnp.dot(arrived, w_gate[0], preferred_element_type=jnp.float32)
    up_pre = jnp.dot(arrived, w_up[0], preferred_element_type=jnp.float32)
    gated = jnp.minimum(gate_pre, 7.0)
    upper = jnp.clip(up_pre, -7.0, 7.0)
    hidden = ((upper + 1.0) * gated * jax.nn.sigmoid(1.702 * gated)).astype(jnp.bfloat16)
    partial_out = jnp.dot(hidden, w_down[0], preferred_element_type=jnp.float32).astype(
        jnp.bfloat16
    )
    summed = (
        lax.psum_scatter(partial_out, "tp", scatter_dimension=1, tiled=True)
        .astype(jnp.float32)
        .astype(jnp.bfloat16)
    )
    returned = lax.all_to_all(
        summed.reshape(groups, capacity, -1), "ep", split_axis=0, concat_axis=0, tiled=True
    ).reshape(slot_rows, -1)
    mixed = jnp.dot(combine, returned.astype(jnp.float32), precision=lax.Precision.HIGHEST)
    return mixed.astype(jnp.bfloat16)


def solution(mesh):
    placed = (
        P("ep", "tp"),
        P("tp"),
        P("ep", None),
        P("ep", None),
        P("ep", None, "tp"),
        P("ep", None, "tp"),
        P("ep", "tp", None),
    )
    return jax.shard_map(
        shards, mesh=mesh, in_specs=placed, out_specs=P("ep", "tp"), check_vma=False
    )
```

profile of v0, /device:TPU:0, one launch (start us, length us, event | category | flops | bytes accessed | tf_op | source)
XLA Modules:
  0.0 120.4 jit_solution(6978321878295605920)
XLA Ops:
  6.5 0.0 reduce-scatter.2.cloned.1.call-start
  6.5 10.1 %all_gather.6 = bf16[16,4096]{1,0:T(8,128)(2,1)S(1)} all-gather(bf16[16,1024]{1,0:T(8,128)(2,1)} %param.7), channel_id=1, replica_groups=mesh['ep'=8,'tp'=4] {'tp'}, dimensions={1}, use_global_device_ids=true | all-gather | bytes 163840 | tf_op jit(solution)/shard_map/all_gather | solution.py:25
  16.7 0.1 fusion.34
  16.8 0.8 copy.21
  17.6 0.1 eq.20
  17.7 0.2 convert_reduce_fusion
  17.9 0.1 reduce_sum.30
  17.9 0.1 copy.22
  18.0 0.7 multiply_add_fusion
  18.7 0.1 fusion.45
  18.8 7.9 %all-gather = bf16[4096]{0:T(1024)(128)(2,1)S(1)} all-gather(bf16[1024]{0:T(1024)(128)(2,1)} %param.8), channel_id=2, replica_groups=mesh['ep'=8,'tp'=4] {'tp'}, dimensions={0}, use_global_device_ids=true | all-gather | bytes 10240 | tf_op jit(solution)/shard_map/all_gather | solution.py:26
  26.7 0.5 convolution_convert_fusion
  27.2 31.2 %all_to_all.10 = bf16[8,16,4096]{2,1,0:T(8,128)(2,1)S(1)} all-to-all(bf16[8,16,4096]{2,1,0:T(8,128)(2,1)S(1)} %bitcast.36), channel_id=1, replica_groups=mesh['ep'=8,'tp'=4] {'ep'}, dimensions={0} | all-to-all | bytes 2097152 | tf_op jit(solution)/shard_map/all_to_all | solution.py:32
  58.4 4.6 %fusion.9 = f32[128,1024]{1,0:T(8,128)S(1)} fusion(bf16[128,4096]{1,0:T(8,128)(2,1)S(1)} %bitcast.34, bf16[1,4096,1024]{2,1,0:T(8,128)(2,1)} %param.11), kind=kOutput, calls=%fused_computation.8 | convolution fusion | flops 1073872896 | bytes 9961472 | tf_op jit(solution)/shard_map/dot_general | solution.py:35
  63.1 0.0 copy-start
  63.1 9.3 %fusion.6 = bf16[128,4096]{1,0:T(8,128)(2,1)} fusion(bf16[1,1024,4096]{2,1,0:T(8,128)(2,1)} %param.13, f32[128,1024]{1,0:T(8,128)S(1)} %fusion.9, bf16[128,4096]{1,0:T(8,128)(2,1)S(1)} %bitcast.35, bf16[1,4096,1024]{2,1,0:T(8,128)(2,1)} %param.12), kind=kOutput, calls=%fused_computation.6 | convolution fusion | flops 2149187584 | bytes 19398656 | tf_op jit(solution)/shard_map/dot_general | solution.py:40
  72.4 0.0 reduce-scatter.2.cloned.1.call-update
  72.4 26.0 %reduce-scatter.2.cloned.1.call-done = bf16[128,1024]{1,0:T(8,128)(2,1)} async-done(((bf16[128,4096]{1,0:T(8,128)(2,1)}), bf16[128,1024]{1,0:T(8,128)(2,1)}) %reduce-scatter.2.cloned.1.call-update) | async-done | bytes 262160 | tf_op jit(solution)/shard_map/reduce_scatter | solution.py:44
  98.4 4.6 %all-to-all-start.1 = ((bf16[8,16,1024]{2,1,0:T(8,128)(2,1)}), bf16[8,16,1024]{2,1,0:T(8,128)(2,1)S(1)}, u32[]{:S(2)}, u32[]{:S(2)}) async-start(bf16[8,16,1024]{2,1,0:T(8,128)(2,1)} %bitcast.38), calls=%async_computation.2 | async-start | bytes 524288 | tf_op jit(solution)/shard_map/all_to_all | solution.py:48
  103.0 0.0 copy-done
  103.1 0.1 select_reduce_fusion
  103.1 9.6 %all-to-all-done.1 = bf16[8,16,1024]{2,1,0:T(8,128)(2,1)S(1)} async-done(((bf16[8,16,1024]{2,1,0:T(8,128)(2,1)}), bf16[8,16,1024]{2,1,0:T(8,128)(2,1)S(1)}, u32[]{:S(2)}, u32[]{:S(2)}) %all-to-all-start.1) | async-done | bytes 262176 | tf_op jit(solution)/shard_map/all_to_all | solution.py:48
  112.8 0.8 convolution_convert_fusion.1
  (2 shorter events, 0.0 us)
Async XLA Ops:
  6.5 91.9 %reduce-scatter.2.cloned.1.call-start = ((), (), s32[]{:S(2)}) async-start(), calls=%async_computation.3 | async-start | bytes 1310720 | tf_op jit(solution)/shard_map/reduce_scatter | solution.py:44
  63.1 40.0 %copy-start = (f32[16,4]{0,1:T(4,128)S(1)}, f32[16,4]{0,1:T(4,128)}, u32[]{:S(2)}) copy-start(f32[16,4]{0,1:T(4,128)} %param.10) | copy-start | bytes 772
  98.4 14.3 %all-to-all-start.1 = ((bf16[8,16,1024]{2,1,0:T(8,128)(2,1)}), bf16[8,16,1024]{2,1,0:T(8,128)(2,1)S(1)}, u32[]{:S(2)}, u32[]{:S(2)}) async-start(bf16[8,16,1024]{2,1,0:T(8,128)(2,1)} %bitcast.38), calls=%async_computation.2 | async-start | bytes 524288 | tf_op jit(solution)/shard_map/all_to_all | solution.py:48
Sparse Core Ops, SparseCore 0:
  72.5 25.8 reduce-scatter.1
where the time goes:
time: 121 us; the launch traced here: 120 us
  blocking collectives  49.2 us (41%)
  waiting for transfers between devices  35.7 us (30%)
  matrix products  15.2 us (13%)
  between operations  13.4 us (11%)
  starting transfers between devices  4.62 us (4%)
    all_to_all x1, blocking collectives, shards(): lax.all_to_all(outbound.reshape(groups, capacity, -1), 'ep', split_axis=0...  31.2 us
    reduce_scatter x1, waiting for transfers between devices, shards(): lax.psum_scatter(partial_out, 'tp', scatter_dimension=1, tiled=True)  26 us
    all_gather x1, blocking collectives, shards(): lax.all_gather(tokens, 'tp', axis=1, tiled=True)  10.1 us
    all_to_all x1, waiting for transfers between devices, shards(): lax.all_to_all(summed.reshape(groups, capacity, -1), 'ep', split_axis=0,...  9.62 us
    dot_general x1, matrix products, shards(): jnp.dot(hidden, w_down[0], preferred_element_type=jnp.float32)  9.29 us
    all_gather x1, blocking collectives, shards(): lax.all_gather(norm_gain.reshape(1, -1), 'tp', axis=1, tiled=True)  7.86 us
    dot_general x1, matrix products, shards(): gate_pre = jnp.dot(arrived, w_gate[0], preferred_element_type=jnp.float32)  4.63 us
    all_to_all x1, starting transfers between devices, shards(): lax.all_to_all(summed.reshape(groups, capacity, -1), 'ep', split_axis=0,...  4.61 us
  transfers between devices with their start and end apart: 2, of which 2 were waited for; matrix products, arithmetic and copies ran while one was open for 0% of the time, Pallas kernels for 0%

commit v1 on v0

--- a/solution.py
+++ b/solution.py
@@ -21,9 +21,15 @@
         jnp.where(target[:, :, None] == slot_ids[None, None, :], route_weights[:, :, None], 0.0),
         axis=1,
     )
+
+    def entries_time(point, axis_k):
+        e_now = lax.all_gather(point, axis_name="tp")
+        mixed_arr = jnp.concatenate(e_now, axis=axis_k)
+        return mixed_arr
+
     whole, gain_whole = (
         lax.all_gather(tokens, "tp", axis=1, tiled=True),
-        lax.all_gather(norm_gain.reshape(1, -1), "tp", axis=1, tiled=True),
+        entries_time(norm_gain.reshape(1, -1), 1),
     )
     full_values = whole.astype(jnp.float32)
     scale = lax.rsqrt(jnp.mean(full_values * full_values, axis=1, keepdims=True) + 1e-05)

time: 121 us -> 121 us (level)
  no operation moved by 1% of the time
where the time goes in v1:
time: 121 us; the launch traced here: 120 us
  blocking collectives  49.2 us (41%)
  waiting for transfers between devices  35.7 us (30%)
  matrix products  15.2 us (13%)
  between operations  13.4 us (11%)
  starting transfers between devices  4.62 us (4%)
    all_to_all x1, blocking collectives, shards(): lax.all_to_all(outbound.reshape(groups, capacity, -1), 'ep', split_axis=0...  31.2 us
    reduce_scatter x1, waiting for transfers between devices, shards(): lax.psum_scatter(partial_out, 'tp', scatter_dimension=1, tiled=True)  26 us
    all_gather x1, blocking collectives, shards(): lax.all_gather(tokens, 'tp', axis=1, tiled=True)  10.1 us
    all_to_all x1, waiting for transfers between devices, shards(): lax.all_to_all(summed.reshape(groups, capacity, -1), 'ep', split_axis=0,...  9.62 us
    dot_general x1, matrix products, shards(): jnp.dot(hidden, w_down[0], preferred_element_type=jnp.float32)  9.29 us
    all_gather x1, blocking collectives, entries_time(): e_now = lax.all_gather(point, axis_name='tp')  7.86 us
    dot_general x1, matrix products, shards(): gate_pre = jnp.dot(arrived, w_gate[0], preferred_element_type=jnp.float32)  4.63 us
    all_to_all x1, starting transfers between devices, shards(): lax.all_to_all(summed.reshape(groups, capacity, -1), 'ep', split_axis=0,...  4.61 us
  transfers between devices with their start and end apart: 2, of which 2 were waited for; matrix products, arithmetic and copies ran while one was open for 0% of the time, Pallas kernels for 0%

profile of v1, /device:TPU:0, one launch (start us, length us, event | category | flops | bytes accessed | tf_op | source)
XLA Modules:
  0.0 120.4 jit_solution(6978321878295605920)
XLA Ops:
  6.5 0.0 reduce-scatter.2.cloned.1.call-start
  6.5 10.1 %all_gather.6 = bf16[16,4096]{1,0:T(8,128)(2,1)S(1)} all-gather(bf16[16,1024]{1,0:T(8,128)(2,1)} %param.7), channel_id=1, replica_groups=mesh['ep'=8,'tp'=4] {'tp'}, dimensions={1}, use_global_device_ids=true | all-gather | bytes 163840 | tf_op jit(solution)/shard_map/all_gather | solution.py:31
  16.7 0.1 fusion.34
  16.8 0.8 copy.21
  17.6 0.1 eq.20
  17.7 0.2 convert_reduce_fusion
  17.9 0.1 reduce_sum.30
  17.9 0.1 copy.22
  18.0 0.7 multiply_add_fusion
  18.7 0.1 fusion.45
  18.8 7.9 %all-gather = bf16[4096]{0:T(1024)(128)(2,1)S(1)} all-gather(bf16[1024]{0:T(1024)(128)(2,1)} %param.8), channel_id=2, replica_groups=mesh['ep'=8,'tp'=4] {'tp'}, dimensions={0}, use_global_device_ids=true | all-gather | bytes 10240 | tf_op jit(solution)/shard_map/all_gather | solution.py:26
  26.7 0.5 convolution_convert_fusion
  27.2 31.2 %all_to_all.10 = bf16[8,16,4096]{2,1,0:T(8,128)(2,1)S(1)} all-to-all(bf16[8,16,4096]{2,1,0:T(8,128)(2,1)S(1)} %bitcast.36), channel_id=1, replica_groups=mesh['ep'=8,'tp'=4] {'ep'}, dimensions={0} | all-to-all | bytes 2097152 | tf_op jit(solution)/shard_map/all_to_all | solution.py:38
  58.4 4.6 %fusion.9 = f32[128,1024]{1,0:T(8,128)S(1)} fusion(bf16[128,4096]{1,0:T(8,128)(2,1)S(1)} %bitcast.34, bf16[1,4096,1024]{2,1,0:T(8,128)(2,1)} %param.11), kind=kOutput, calls=%fused_computation.8 | convolution fusion | flops 1073872896 | bytes 9961472 | tf_op jit(solution)/shard_map/dot_general | solution.py:41
  63.1 0.0 copy-start
  63.1 9.3 %fusion.6 = bf16[128,4096]{1,0:T(8,128)(2,1)} fusion(bf16[1,1024,4096]{2,1,0:T(8,128)(2,1)} %param.13, f32[128,1024]{1,0:T(8,128)S(1)} %fusion.9, bf16[128,4096]{1,0:T(8,128)(2,1)S(1)} %bitcast.35, bf16[1,4096,1024]{2,1,0:T(8,128)(2,1)} %param.12), kind=kOutput, calls=%fused_computation.6 | convolution fusion | flops 2149187584 | bytes 19398656 | tf_op jit(solution)/shard_map/dot_general | solution.py:46
  72.4 0.0 reduce-scatter.2.cloned.1.call-update
  72.4 26.0 %reduce-scatter.2.cloned.1.call-done = bf16[128,1024]{1,0:T(8,128)(2,1)} async-done(((bf16[128,4096]{1,0:T(8,128)(2,1)}), bf16[128,1024]{1,0:T(8,128)(2,1)}) %reduce-scatter.2.cloned.1.call-update) | async-done | bytes 262160 | tf_op jit(solution)/shard_map/reduce_scatter | solution.py:50
  98.4 4.6 %all-to-all-start.1 = ((bf16[8,16,1024]{2,1,0:T(8,128)(2,1)}), bf16[8,16,1024]{2,1,0:T(8,128)(2,1)S(1)}, u32[]{:S(2)}, u32[]{:S(2)}) async-start(bf16[8,16,1024]{2,1,0:T(8,128)(2,1)} %bitcast.38), calls=%async_computation.2 | async-start | bytes 524288 | tf_op jit(solution)/shard_map/all_to_all | solution.py:54
  103.0 0.0 copy-done
  103.1 0.1 select_reduce_fusion
  103.1 9.6 %all-to-all-done.1 = bf16[8,16,1024]{2,1,0:T(8,128)(2,1)S(1)} async-done(((bf16[8,16,1024]{2,1,0:T(8,128)(2,1)}), bf16[8,16,1024]{2,1,0:T(8,128)(2,1)S(1)}, u32[]{:S(2)}, u32[]{:S(2)}) %all-to-all-start.1) | async-done | bytes 262176 | tf_op jit(solution)/shard_map/all_to_all | solution.py:54
  112.8 0.8 convolution_convert_fusion.1
  (2 shorter events, 0.0 us)
Async XLA Ops:
  6.5 91.9 %reduce-scatter.2.cloned.1.call-start = ((), (), s32[]{:S(2)}) async-start(), calls=%async_computation.3 | async-start | bytes 1310720 | tf_op jit(solution)/shard_map/reduce_scatter | solution.py:50
  63.1 40.0 %copy-start = (f32[16,4]{0,1:T(4,128)S(1)}, f32[16,4]{0,1:T(4,128)}, u32[]{:S(2)}) copy-start(f32[16,4]{0,1:T(4,128)} %param.10) | copy-start | bytes 772
  98.4 14.3 %all-to-all-start.1 = ((bf16[8,16,1024]{2,1,0:T(8,128)(2,1)}), bf16[8,16,1024]{2,1,0:T(8,128)(2,1)S(1)}, u32[]{:S(2)}, u32[]{:S(2)}) async-start(bf16[8,16,1024]{2,1,0:T(8,128)(2,1)} %bitcast.38), calls=%async_computation.2 | async-start | bytes 524288 | tf_op jit(solution)/shard_map/all_to_all | solution.py:54
Sparse Core Ops, SparseCore 0:
  72.5 25.8 reduce-scatter.1
